TPU v7x, 128 devices: a whole 4x4x4 slice. The times are simulated.
128 devices in a mesh: sp: 16 (over z, y), tp: 8 (over x, core).
Axes of the slice: x: 4, y: 4, z: 4, core: 2. Of those that a mesh axis runs over, the one named last changes fastest.
Arguments:
- queries: bfloat16 [12288, 2048], P('sp', 'tp'), may hold values from -11 to 11
- key_rows: bfloat16 [12288, 2048], P('sp', 'tp'), may hold values from -4.5 to 4.5
- value_rows: bfloat16 [12288, 2048], P('sp', 'tp'), may hold values from -6 to 6
- log_forget: float32 [12288, 32], P('sp', 'tp'), may hold values from -1477.56 to 0, as said below
- stream_in: bfloat16 [12288, 2048], P('sp'), may hold values from -6 to 6
- out_weight: bfloat16 [2048, 2048], P('tp'), may hold values from -0.52734375 to 0.52734375
- mix_gain: float32 [2048], replicated, may hold values from 0.1 to 1.9
- mix_bias: float32 [2048], replicated, may hold values from -3 to 3
- gate_weight: bfloat16 [2048, 5632], P('sp', 'tp'), may hold values from -0.125 to 0.125
- up_weight: bfloat16 [2048, 5632], P('sp', 'tp'), may hold values from -0.125 to 0.125
- down_weight: bfloat16 [5632, 2048], P('tp', 'sp'), may hold values from -0.15917969 to 0.15917969
- ffn_gain: float32 [2048], replicated, may hold values from 0.1 to 1.9
- ffn_bias: float32 [2048], replicated, may hold values from -3 to 3
Outputs:
- layer_out: bfloat16 [12288, 2048], P(('sp', 'tp'))
Inputs may be any that keep to these rules, and one draw needn't show every extreme that they name: `log_forget`: each column never rises along the positions.
All inputs are finite; a program needn't handle non-finite values.
Results may differ from a plain program's by a relative error of at most 0.015.
Values may be sent and summed in bfloat16 or wider, within the bound.
A program may use at most 128 MiB of HBM per device.

v0:
```python
import jax
import jax.numpy as jnp
from jax import lax
from jax.sharding import PartitionSpec as P

ALPHA = 8.0**0.25
EPSILON = 1e-05


def laid_out(pieces, dim):
    lengths = list(pieces.shape[1:])
    lengths[dim] *= pieces.shape[0]
    return jnp.moveaxis(pieces, 0, dim).reshape(lengths)


def from_everyone(value, axis):
    copies = jnp.broadcast_to(value, (lax.axis_size(axis), *value.shape))
    return lax.all_to_all(copies, axis, split_axis=0, concat_axis=0, tiled=True)


def gathered_copies(value, axis, dim):
    return laid_out(from_everyone(value, axis), dim)


def in_one_piece(arrays, axis, dim, along):
    ends, at = ([], 0)
    for a in arrays[:-1]:
        at += a.shape[along]
        ends.append(at)
    both = jnp.concatenate(arrays, axis=along)
    return tuple(jnp.split(lax.all_gather(both, axis, axis=dim, tiled=True), ends, axis=along))


def in_blocks(value, dim, count):
    before, after = (value.shape[:dim], value.shape[dim + 1 :])
    return jnp.moveaxis(value.reshape(*before, count, -1, *after), dim, 0)


def sum_at_owner(value, axis, dim):
    pieces = in_blocks(value, dim, lax.axis_size(axis))
    arrived = lax.all_to_all(pieces, axis, split_axis=0, concat_axis=0, tiled=True)
    return arrived.astype(jnp.float32).sum(axis=0)


def layer_norm(matrix, norm_gain, norm_shift):
    centred = matrix - jnp.mean(matrix, axis=-1, keepdims=True)
    spread = jnp.mean(centred * centred, axis=-1, keepdims=True)
    return centred * lax.rsqrt(spread + EPSILON) * norm_gain + norm_shift


def attend(queries, key_rows, value_rows, log_forget):
    length, row_width = queries.shape
    head_count = log_forget.shape[1]
    head_dim = row_width // head_count
    score_scale = head_dim ** (-0.5)
    first_pos = lax.axis_index("sp") * length
    last_pos = first_pos + length
    query_heads = queries.reshape(length, head_count, head_dim)
    query_gates = log_forget.T
    query_pos = first_pos + jnp.arange(length, dtype=jnp.int32)
    gates_all = gathered_copies(log_forget, "sp", 0)
    initial = (
        jnp.full((head_count, length), -1e30, jnp.float32),
        jnp.zeros((head_count, length), jnp.float32),
        jnp.zeros((length, head_count, head_dim), jnp.float32),
    )
    running = initial
    key_piece, value_piece = in_one_piece((key_rows, value_rows), "sp", 0, 1)
    piece_len = key_piece.shape[0]
    shards = piece_len // length
    group_size = max(
        [
            count_try
            for count_try in range(1, shards + 1)
            if shards % count_try == 0 and count_try * length <= max(length, 512)
        ]
    )
    block_len = group_size * length
    blocks = piece_len // block_len
    key_blocks = key_piece.reshape(blocks, block_len, head_count, head_dim)
    value_blocks = value_piece.reshape(blocks, block_len, head_count, head_dim)
    gate_blocks = gates_all.reshape(blocks, block_len, head_count)
    block_starts = block_len * jnp.arange(blocks, dtype=jnp.int32)

    def one_block(running_state, packed):
        key_block, value_block, gate_block, block_start = packed

        def compute(state_in):
            highest, totals, weighted = state_in
            scores = (
                jnp.einsum(
                    "qhd,khd->hqk", query_heads, key_block, preferred_element_type=jnp.float32
                )
                * score_scale
            )
            scores = scores + query_gates[:, :, None] - gate_block.T[:, None, :]
            key_pos = block_start + jnp.arange(block_len, dtype=jnp.int32)
            allowed = (key_pos[None, :] <= query_pos[:, None])[None]
            masked = jnp.where(allowed, scores, -1e30)
            new_high = jnp.maximum(highest, jnp.max(masked, axis=2))
            weights = jnp.where(allowed, jnp.exp(masked - new_high[:, :, None]), 0.0)
            factor = jnp.exp(highest - new_high)
            totals = totals * factor + jnp.sum(weights, axis=2)
            weighted = weighted * factor.T[:, :, None] + jnp.einsum(
                "hqk,khd->qhd",
                weights.astype(jnp.bfloat16),
                value_block,
                preferred_element_type=jnp.float32,
            )
            return (new_high, totals, weighted)

        def keep_state(state_in):
            return state_in

        return (lax.cond(block_start < last_pos, compute, keep_state, running_state), None)

    running, unused = lax.scan(
        one_block, running, (key_blocks, value_blocks, gate_blocks, block_starts)
    )
    highest, totals, weighted = running
    return (weighted / totals.T[:, :, None]).reshape(length, row_width).astype(jnp.bfloat16)


def body(
    queries,
    key_rows,
    value_rows,
    log_forget,
    stream_in,
    out_weight,
    mix_gain,
    mix_bias,
    gate_weight,
    up_weight,
    down_weight,
    ffn_gain,
    ffn_bias,
):
    attended = attend(queries, key_rows, value_rows, log_forget)
    length = attended.shape[0]
    own_rows = length // lax.axis_size("tp")
    offset = lax.axis_index("tp") * own_rows
    summed = sum_at_owner(
        jnp.dot(attended, out_weight, preferred_element_type=jnp.float32).astype(jnp.bfloat16),
        "tp",
        0,
    )
    mix_out = lax.optimization_barrier(summed.astype(jnp.bfloat16)).astype(jnp.float32)
    stream_own = lax.dynamic_slice_in_dim(stream_in, offset, own_rows, 0)
    normed = layer_norm(
        ALPHA * stream_own.astype(jnp.float32) + mix_out, mix_gain, mix_bias
    ).astype(jnp.bfloat16)
    gathered = lax.all_gather(normed, "tp", axis=0, tiled=True)
    pieces = in_one_piece((gate_weight, up_weight), "sp", 0, 1)
    gate_part = jnp.dot(gathered, pieces[0], preferred_element_type=jnp.float32)
    up_part = jnp.dot(gathered, pieces[1], preferred_element_type=jnp.float32)
    hidden = (jax.nn.silu(gate_part) * up_part).astype(jnp.bfloat16)
    partial_terms = jnp.dot(
        hidden,
        lax.all_gather(down_weight, "sp", axis=1, tiled=True),
        preferred_element_type=jnp.float32,
    )
    lowered = lax.psum_scatter(
        partial_terms.astype(jnp.bfloat16), "tp", scatter_dimension=0, tiled=True
    ).astype(jnp.float32)
    lowered = lax.optimization_barrier(lowered.astype(jnp.bfloat16)).astype(jnp.float32)
    result = layer_norm(ALPHA * normed.astype(jnp.float32) + lowered, ffn_gain, ffn_bias)
    return result.astype(jnp.bfloat16)


def solution(mesh):
    placed = (
        P("sp", "tp"),
        P("sp", "tp"),
        P("sp", "tp"),
        P("sp", "tp"),
        P("sp", None),
        P("tp", None),
        P(),
        P(),
        P("sp", "tp"),
        P("sp", "tp"),
        P("tp", "sp"),
        P(),
        P(),
    )
    return jax.shard_map(
        body, mesh=mesh, in_specs=placed, out_specs=P(("sp", "tp"), None), check_vma=False
    )
```

profile of v0, /device:TPU:0, one launch (start us, length us, event | category | flops | bytes accessed | tf_op | source)
XLA Modules:
  0.0 604.3 jit_solution(4880820120093457124)
XLA Ops:
  6.5 2.2 pad_maximum_fusion
  8.7 0.0 all-gather.5.cloned.1.call-update
  8.8 0.0 all-gather.9.cloned.1.call-start
  8.8 1.8 pad_maximum_fusion.1
  10.6 0.0 all-gather.9.cloned.1.call-update
  10.6 1.4 broadcast_in_dim.56
  12.0 8.2 %all-to-all-start = ((f32[16,768,4]{1,2,0:T(4,128)}), f32[16,768,4]{1,2,0:T(4,128)S(1)}, u32[]{:S(2)}, u32[]{:S(2)}) async-start(f32[16,768,4]{1,2,0:T(4,128)} %broadcast_in_dim.56), calls=%async_computation | async-start | bytes 393216 | tf_op jit(solution)/shard_map/all_to_all | solution.py:18
  20.2 1.2 copy.18
  21.4 80.5 %all-gather.5.cloned.1.call-done = bf16[12288,512]{1,0:T(8,128)(2,1)} async-done(((bf16[768,512]{1,0:T(8,128)(2,1)}), bf16[12288,512]{1,0:T(8,128)(2,1)}) %all-gather.5.cloned.1.call-update) | async-done | bytes 12582928 | tf_op jit(solution)/shard_map/all_gather | solution.py:31
  101.9 10.1 %fusion.36 = (bf16[12288,256]{1,0:T(8,128)(2,1)}, bf16[12288,256]{1,0:T(8,128)(2,1)}) fusion(bf16[12288,512]{1,0:T(8,128)(2,1)} %all-gather.5.cloned.1.call-done), kind=kLoop, calls=%fused_computation.51 | loop fusion | bytes 25165824 | tf_op jit(solution)/shard_map/split | solution.py:31
  112.0 18.8 %reshape.82 = bf16[16,768,4,64]{3,2,1,0:T(4,128)(2,1)} reshape(bf16[12288,256]{1,0:T(8,128)(2,1)} %get-tuple-element.249) | data formatting | bytes 12582912 | tf_op jit(solution)/shard_map/reshape | solution.py:80
  130.8 18.1 %copy.20 = bf16[16,768,4,64]{1,3,2,0:T(8,128)(2,1)} copy(bf16[16,768,4,64]{3,2,1,0:T(4,128)(2,1)} %reshape.82) | data formatting | bytes 12582912
  148.9 18.8 %reshape.83 = bf16[16,768,4,64]{3,2,1,0:T(4,128)(2,1)} reshape(bf16[12288,256]{1,0:T(8,128)(2,1)} %get-tuple-element.248) | data formatting | bytes 12582912 | tf_op jit(solution)/shard_map/reshape | solution.py:81
  167.6 18.1 %copy.21 = bf16[16,768,4,64]{1,3,2,0:T(8,128)(2,1)} copy(bf16[16,768,4,64]{3,2,1,0:T(4,128)(2,1)} %reshape.83) | data formatting | bytes 12582912
  185.7 0.0 all-to-all-done
  185.7 0.1 broadcast_in_dim.55
  185.8 33.5 %while.15 = (s32[]{:T(128)}, f32[4,768]{1,0:T(4,128)S(1)}, f32[4,768]{1,0:T(4,128)S(1)}, f32[768,4,64]{0,2,1:T(8,128)S(1)}, s32[16]{0:T(128)S(1)}, /*index=5*/s3...) while((s32[]{:T(128)}, f32[4,768]{1,0:T(4,128)S(1)}, ...), condition=%wide.region_5.6_spmd.clone, body=%wide.region_0.5_spmd.clone.sunk | while | flops 649800192 | bytes 33738040 | solution.py:117
  185.8 0.6 dynamic_slice.50
  187.1 13.1 %conditional.3 = ((f32[4,768]{1,0:T(4,128)S(1)}, f32[4,768]{1,0:T(4,128)S(1)}, f32[768,4,64]{0,2,1:T(8,128)S(1)})) conditional(s32[]{:T(128)} %convert_element_type.100, (f32[4,768]{1,0:T(4,128)S(1)}, f32[4,768]{1,0:T(4,128)S(1)}, f32[768,4,64]{0,2,1:T(8,128)S(1)}) %tuple.41, (s32[]{:T(128)}, s32[]{:T(128)}, bf16[16,768,4,64]{1,3,2,0:T(8,128)(2,1)}, ...), branch_computations={%region_1.1_spmd, %region_2.4_spmd} | conditional | flops 649800192 | bytes 33734700 | solution.py:115
  187.1 0.7 iota_add_fusion
  187.7 0.4 broadcast_compare_fusion
  188.2 3.9 fusion.4
  192.0 4.6 fusion.11
  196.6 3.5 fusion.3
  200.2 0.6 dynamic_slice.50
  201.4 0.6 dynamic_slice.50
  202.7 0.6 dynamic_slice.50
  204.0 0.6 dynamic_slice.50
  205.3 0.6 dynamic_slice.50
  206.5 0.6 dynamic_slice.50
  207.8 0.6 dynamic_slice.50
  209.1 0.6 dynamic_slice.50
  210.4 0.6 dynamic_slice.50
  211.7 0.6 dynamic_slice.50
  212.9 0.6 dynamic_slice.50
  214.2 0.6 dynamic_slice.50
  215.5 0.6 dynamic_slice.50
  216.8 0.6 dynamic_slice.50
  218.0 0.6 dynamic_slice.50
  219.3 0.1 divide_convert_fusion
  219.4 0.0 copy-done
  219.4 2.7 convolution_convert_fusion.1
  222.1 4.6 all-to-all-start.1
  226.7 0.2 all-gather.7.cloned.1.call-start
  226.9 38.2 %all-to-all-done.1 = bf16[8,96,2048]{2,1,0:T(8,128)(2,1)} async-done(((bf16[8,96,2048]{2,1,0:T(8,128)(2,1)}), bf16[8,96,2048]{2,1,0:T(8,128)(2,1)}, u32[]{:S(2)}, u32[]{:S(2)}) %all-to-all-start.1) | async-done | bytes 3145760 | tf_op jit(solution)/shard_map/all_to_all | solution.py:41
  265.1 2.5 reduce_sum.59
  267.6 1.2 fusion.33
  268.8 1.3 multiply_reduce_fusion.1
  270.2 2.0 add_convert_fusion.1
  272.2 0.0 all-gather.7.cloned.1.call-update
  272.2 0.0 all-gather.11.cloned.1.call-start
  272.2 0.5 all-gather.11.cloned.1.call-update
  272.8 0.0 reduce-scatter.2.cloned.1.call-start
  272.8 0.0 all-gather.9.cloned.1.call-done
  272.8 220.0 %all-gather.7.cloned.1.call-done = bf16[768,2048]{1,0:T(8,128)(2,1)} async-done(((bf16[96,2048]{1,0:T(8,128)(2,1)}), bf16[768,2048]{1,0:T(8,128)(2,1)}) %all-gather.7.cloned.1.call-update) | async-done | bytes 3145744 | tf_op jit(solution)/shard_map/all_gather | solution.py:153
  492.8 6.5 %fusion.27 = f32[768,704]{0,1:T(8,128)} fusion(bf16[768,2048]{1,0:T(8,128)(2,1)} %all-gather.7.cloned.1.call-done, bf16[2048,1408]{0,1:T(8,128)(2,1)} %all-gather.9.cloned.1.call-done), kind=kOutput, calls=%fused_computation.31 | convolution fusion | flops 2214592512 | bytes 8192000 | tf_op jit(solution)/shard_map/dot_general | solution.py:155
  499.3 46.2 %all-gather.11.cloned.1.call-done = bf16[704,2048]{1,0:T(8,128)(2,1)} async-done(((bf16[704,128]{1,0:T(8,128)(2,1)}), bf16[704,2048]{1,0:T(8,128)(2,1)}) %all-gather.11.cloned.1.call-update) | async-done | bytes 2883600 | tf_op jit(solution)/shard_map/all_gather | solution.py:160
  545.5 12.4 %convolution_convert_fusion = bf16[768,2048]{1,0:T(8,128)(2,1)} fusion(bf16[704,2048]{1,0:T(8,128)(2,1)} %all-gather.11.cloned.1.call-done, f32[768,704]{0,1:T(8,128)} %fusion.27, bf16[768,2048]{1,0:T(8,128)(2,1)} %all-gather.7.cloned.1.call-done, bf16[2048,1408]{0,1:T(8,128)(2,1)} %all-gather.9.cloned.1.call-done), kind=kOutput, calls=%fused_computation.27 | convolution fusion | flops 4434001920 | bytes 14221312 | tf_op jit(solution)/shard_map/dot_general | solution.py:158
  557.9 0.0 reduce-scatter.2.cloned.1.call-update
  557.9 35.3 %reduce-scatter.2.cloned.1.call-done = bf16[96,2048]{1,0:T(8,128)(2,1)} async-done(((bf16[768,2048]{1,0:T(8,128)(2,1)}), bf16[96,2048]{1,0:T(8,128)(2,1)}) %reduce-scatter.2.cloned.1.call-update) | async-done | bytes 393232 | tf_op jit(solution)/shard_map/reduce_scatter | solution.py:163
  593.2 0.0 copy-done.1
  593.2 1.2 fusion.34
  594.4 1.3 multiply_reduce_fusion
  595.7 2.0 add_convert_fusion
  (55 shorter events, 0.3 us)
Async XLA Ops:
  6.5 212.9 %copy-start = (bf16[256,2048]{1,0:T(8,128)(2,1)S(1)}, bf16[256,2048]{1,0:T(8,128)(2,1)}, u32[]{:S(2)}) copy-start(bf16[256,2048]{1,0:T(8,128)(2,1)} %param.22) | copy-start | bytes 3145732
  6.5 95.4 %all-gather.5.cloned.1.call-start = ((), (), s32[]{:S(2)}) async-start(), calls=%async_computation.3 | async-start | bytes 13369344 | tf_op jit(solution)/shard_map/all_gather | solution.py:31
  8.8 264.1 %all-gather.9.cloned.1.call-start = ((), (), s32[]{:S(2)}) async-start(), calls=%async_computation.5 | async-start | bytes 6127616 | tf_op jit(solution)/shard_map/all_gather | solution.py:31
  12.0 173.7 %all-to-all-start = ((f32[16,768,4]{1,2,0:T(4,128)}), f32[16,768,4]{1,2,0:T(4,128)S(1)}, u32[]{:S(2)}, u32[]{:S(2)}) async-start(f32[16,768,4]{1,2,0:T(4,128)} %broadcast_in_dim.56), calls=%async_computation | async-start | bytes 393216 | tf_op jit(solution)/shard_map/all_to_all | solution.py:18
  167.6 18.2 %copy-start.2 = (f32[768,4]{0,1:T(4,128)S(1)}, f32[768,4]{0,1:T(4,128)}, u32[]{:S(2)}) copy-start(f32[768,4]{0,1:T(4,128)} %param.20) | copy-start | bytes 36868
  222.1 48.0 %copy-start.3 = (f32[2048]{0:T(1024)S(1)}, f32[2048]{0:T(1024)}, u32[]{:S(2)}) copy-start(f32[2048]{0:T(1024)} %param.24) | copy-start | bytes 24580
  222.1 48.0 %copy-start.4 = (f32[2048]{0:T(1024)S(1)}, f32[2048]{0:T(1024)}, u32[]{:S(2)}) copy-start(f32[2048]{0:T(1024)} %param.23) | copy-start | bytes 24580
  222.1 43.0 %all-to-all-start.1 = ((bf16[8,96,2048]{2,1,0:T(8,128)(2,1)}), bf16[8,96,2048]{2,1,0:T(8,128)(2,1)}, u32[]{:S(2)}, u32[]{:S(2)}) async-start(bf16[8,96,2048]{2,1,0:T(8,128)(2,1)} %bitcast.45), calls=%async_computation.1 | async-start | bytes 6291456 | tf_op jit(solution)/shard_map/all_to_all | solution.py:41
  226.7 266.1 %all-gather.7.cloned.1.call-start = ((), (), s32[]{:S(2)}) async-start(), calls=%async_computation.4 | async-start | bytes 3538944 | tf_op jit(solution)/shard_map/all_gather | solution.py:153
  272.2 273.3 %all-gather.11.cloned.1.call-start = ((), (), s32[]{:S(2)}) async-start(), calls=%async_computation.6 | async-start | bytes 3063808 | tf_op jit(solution)/shard_map/all_gather | solution.py:160
  272.8 320.4 %reduce-scatter.2.cloned.1.call-start = ((), (), s32[]{:S(2)}) async-start(), calls=%async_computation.7 | async-start | bytes 3538944 | tf_op jit(solution)/shard_map/reduce_scatter | solution.py:163
  499.3 93.9 %copy-start.1 = (bf16[96,2048]{1,0:T(8,128)(2,1)S(1)}, bf16[96,2048]{1,0:T(8,128)(2,1)}, u32[]{:S(2)}) copy-start(bf16[96,2048]{1,0:T(8,128)(2,1)} %add_convert_fusion.1) | copy-start | bytes 1179652
  499.3 96.4 %copy-start.5 = (f32[2048]{0:T(1024)S(1)}, f32[2048]{0:T(1024)}, u32[]{:S(2)}) copy-start(f32[2048]{0:T(1024)} %param.29) | copy-start | bytes 24580
  499.3 96.4 %copy-start.6 = (f32[2048]{0:T(1024)S(1)}, f32[2048]{0:T(1024)}, u32[]{:S(2)}) copy-start(f32[2048]{0:T(1024)} %param.28) | copy-start | bytes 24580
Sparse Core Ops, SparseCore 0:
  9.5 92.3 all-gather.4
  104.0 64.0 all-gather.8
  272.3 220.4 all-gather.6
  494.8 50.6 all-gather.10
  558.0 35.0 reduce-scatter.1
where the time goes:
time: 608 us; the launch traced here: 604 us
  waiting for transfers between devices  421 us (69%)
  local copies, waits for them, and re-layouts  95.9 us (16%)
  matrix products  30.1 us (5%)
  other arithmetic  20.1 us (3%)
  between operations  13.3 us (2%)
  starting transfers between devices  13.1 us (2%)
  loops' own time  11.1 us (2%)
    all_gather x1, waiting for transfers between devices, body(): gathered = lax.all_gather(normed, 'tp', axis=0, tiled=True)  220 us
    all_gather x2, waiting for transfers between devices, in_one_piece(): lax.all_gather(both, axis, axis=dim, tiled=True)  80.5 us
    all_gather x1, waiting for transfers between devices, body(): lax.all_gather(down_weight, 'sp', axis=1, tiled=True)  46.2 us
    all_to_all x1, waiting for transfers between devices, sum_at_owner(): lax.all_to_all(pieces, axis, split_axis=0, concat_axis=0, tiled=True)  38.2 us
    unnamed x17, local copies, waits for them, and re-layouts  37.4 us
    reduce_scatter x1, waiting for transfers between devices, body(): lax.psum_scatter(partial_terms.astype(jnp.bfloat16), 'tp', scatter_dimens...  35.3 us
    reshape x1, local copies, waits for them, and re-layouts, attend(): key_blocks = key_piece.reshape(blocks, block_len, head_count, head_dim)  18.8 us
    reshape x1, local copies, waits for them, and re-layouts, attend(): value_blocks = value_piece.reshape(blocks, block_len, head_count, head_dim)  18.8 us
  transfers between devices with their start and end apart: 7, of which 5 were waited for; matrix products, arithmetic and copies ran while one was open for 21% of the time, Pallas kernels for 0%

commit v1 on v0

--- a/solution.py
+++ b/solution.py
@@ -157,7 +157,7 @@
     hidden = (jax.nn.silu(gate_part) * up_part).astype(jnp.bfloat16)
     partial_terms = jnp.dot(
         hidden,
-        lax.all_gather(down_weight, "sp", axis=1, tiled=True),
+        jnp.concatenate(lax.all_gather(down_weight, "sp"), axis=1),
         preferred_element_type=jnp.float32,
     )
     lowered = lax.psum_scatter(

time: 608 us -> 563 us (0.926)
  waiting for transfers between devices: 421 us -> 371 us
    all_gather x1, waiting for transfers between devices: 46.2 us -> 0.02 us  [body(): lax.all_gather(down_weight, 'sp')]
  transfers between devices with their start and end apart: 7 -> 7, of which waited for: 5 -> 4; matrix products, arithmetic and copies ran while one was open for 21% -> 22% of each run, Pallas kernels for 0% -> 0%
where the time goes in v1:
time: 563 us; the launch traced here: 560 us
  waiting for transfers between devices  371 us (66%)
  local copies, waits for them, and re-layouts  101 us (18%)
  matrix products  30.2 us (5%)
  other arithmetic  20.1 us (4%)
  between operations  13.3 us (2%)
  starting transfers between devices  13.1 us (2%)
  loops' own time  11.1 us (2%)
    all_gather x1, waiting for transfers between devices, body(): gathered = lax.all_gather(normed, 'tp', axis=0, tiled=True)  215 us
    all_gather x2, waiting for transfers between devices, in_one_piece(): lax.all_gather(both, axis, axis=dim, tiled=True)  80.2 us
    all_to_all x1, waiting for transfers between devices, sum_at_owner(): lax.all_to_all(pieces, axis, split_axis=0, concat_axis=0, tiled=True)  38.2 us
    unnamed x17, local copies, waits for them, and re-layouts  37.5 us
    reduce_scatter x1, waiting for transfers between devices, body(): lax.psum_scatter(partial_terms.astype(jnp.bfloat16), 'tp', scatter_dimens...  36.1 us
    reshape x1, local copies, waits for them, and re-layouts, attend(): value_blocks = value_piece.reshape(blocks, block_len, head_count, head_dim)  18.7 us
    reshape x1, local copies, waits for them, and re-layouts, attend(): key_blocks = key_piece.reshape(blocks, block_len, head_count, head_dim)  18.7 us
    dot_general x1, matrix products, body(): jnp.dot(hidden, jnp.concatenate(lax.all_gather(down_weight, 'sp'), axis=1...  12.5 us
  transfers between devices with their start and end apart: 7, of which 4 were waited for; matrix products, arithmetic and copies ran while one was open for 22% of the time, Pallas kernels for 0%

profile of v1, /device:TPU:0, one launch (start us, length us, event | category | flops | bytes accessed | tf_op | source)
XLA Modules:
  0.0 559.6 jit_solution(8461673568694545739)
XLA Ops:
  6.5 2.2 pad_maximum_fusion
  8.7 0.0 all-gather.6.cloned.1.call-update
  8.8 0.0 all-gather.12.cloned.1.call-start
  8.8 0.7 all-gather.12.cloned.1.call-update
  9.5 0.0 all-gather.10.cloned.1.call-start
  9.6 1.8 pad_maximum_fusion.1
  11.3 0.0 all-gather.10.cloned.1.call-update
  11.3 1.4 broadcast_in_dim.56
  12.8 8.2 %all-to-all-start = ((f32[16,768,4]{1,2,0:T(4,128)}), f32[16,768,4]{1,2,0:T(4,128)S(1)}, u32[]{:S(2)}, u32[]{:S(2)}) async-start(f32[16,768,4]{1,2,0:T(4,128)} %broadcast_in_dim.56), calls=%async_computation | async-start | bytes 393216 | tf_op jit(solution)/shard_map/all_to_all | solution.py:18
  20.9 1.2 copy.18
  22.2 80.2 %all-gather.6.cloned.1.call-done = bf16[12288,512]{1,0:T(8,128)(2,1)} async-done(((bf16[768,512]{1,0:T(8,128)(2,1)}), bf16[12288,512]{1,0:T(8,128)(2,1)}) %all-gather.6.cloned.1.call-update) | async-done | bytes 12582928 | tf_op jit(solution)/shard_map/all_gather | solution.py:31
  102.4 10.1 %fusion.38 = (bf16[12288,256]{1,0:T(8,128)(2,1)}, bf16[12288,256]{1,0:T(8,128)(2,1)}) fusion(bf16[12288,512]{1,0:T(8,128)(2,1)} %all-gather.6.cloned.1.call-done), kind=kLoop, calls=%fused_computation.53 | loop fusion | bytes 25165824 | tf_op jit(solution)/shard_map/split | solution.py:31
  112.5 18.7 %reshape.91 = bf16[16,768,4,64]{3,2,1,0:T(4,128)(2,1)} reshape(bf16[12288,256]{1,0:T(8,128)(2,1)} %get-tuple-element.249) | data formatting | bytes 12582912 | tf_op jit(solution)/shard_map/reshape | solution.py:80
  131.1 18.2 %copy.20 = bf16[16,768,4,64]{1,3,2,0:T(8,128)(2,1)} copy(bf16[16,768,4,64]{3,2,1,0:T(4,128)(2,1)} %reshape.91) | data formatting | bytes 12582912
  149.3 18.7 %reshape.92 = bf16[16,768,4,64]{3,2,1,0:T(4,128)(2,1)} reshape(bf16[12288,256]{1,0:T(8,128)(2,1)} %get-tuple-element.248) | data formatting | bytes 12582912 | tf_op jit(solution)/shard_map/reshape | solution.py:81
  168.0 18.1 %copy.21 = bf16[16,768,4,64]{1,3,2,0:T(8,128)(2,1)} copy(bf16[16,768,4,64]{3,2,1,0:T(4,128)(2,1)} %reshape.92) | data formatting | bytes 12582912
  186.2 0.0 all-to-all-done
  186.2 0.1 broadcast_in_dim.55
  186.3 0.0 copy-done.2
  186.3 33.5 %while.15 = (s32[]{:T(128)}, f32[4,768]{1,0:T(4,128)S(1)}, f32[4,768]{1,0:T(4,128)S(1)}, f32[768,4,64]{0,2,1:T(8,128)S(1)}, s32[16]{0:T(128)S(1)}, /*index=5*/s3...) while((s32[]{:T(128)}, f32[4,768]{1,0:T(4,128)S(1)}, ...), condition=%wide.region_5.6_spmd.clone, body=%wide.region_0.5_spmd.clone.sunk | while | flops 649800192 | bytes 33738040 | solution.py:117
  186.3 0.6 dynamic_slice.50
  187.5 13.1 %conditional.3 = ((f32[4,768]{1,0:T(4,128)S(1)}, f32[4,768]{1,0:T(4,128)S(1)}, f32[768,4,64]{0,2,1:T(8,128)S(1)})) conditional(s32[]{:T(128)} %convert_element_type.100, (f32[4,768]{1,0:T(4,128)S(1)}, f32[4,768]{1,0:T(4,128)S(1)}, f32[768,4,64]{0,2,1:T(8,128)S(1)}) %tuple.41, (s32[]{:T(128)}, s32[]{:T(128)}, bf16[16,768,4,64]{1,3,2,0:T(8,128)(2,1)}, ...), branch_computations={%region_1.1_spmd, %region_2.4_spmd} | conditional | flops 649800192 | bytes 33734700 | solution.py:115
  187.6 0.7 iota_add_fusion
  188.2 0.4 broadcast_compare_fusion
  188.6 3.9 fusion.4
  192.5 4.6 fusion.11
  197.1 3.5 fusion.3
  200.6 0.6 dynamic_slice.50
  201.9 0.6 dynamic_slice.50
  203.2 0.6 dynamic_slice.50
  204.5 0.6 dynamic_slice.50
  205.8 0.6 dynamic_slice.50
  207.0 0.6 dynamic_slice.50
  208.3 0.6 dynamic_slice.50
  209.6 0.6 dynamic_slice.50
  210.9 0.6 dynamic_slice.50
  212.2 0.6 dynamic_slice.50
  213.4 0.6 dynamic_slice.50
  214.7 0.6 dynamic_slice.50
  216.0 0.6 dynamic_slice.50
  217.3 0.6 dynamic_slice.50
  218.5 0.6 dynamic_slice.50
  219.8 0.1 divide_convert_fusion
  219.9 0.0 copy-done
  219.9 2.7 convolution_convert_fusion.1
  222.6 4.6 all-to-all-start.1
  227.2 0.2 all-gather.8.cloned.1.call-start
  227.4 38.2 %all-to-all-done.1 = bf16[8,96,2048]{2,1,0:T(8,128)(2,1)} async-done(((bf16[8,96,2048]{2,1,0:T(8,128)(2,1)}), bf16[8,96,2048]{2,1,0:T(8,128)(2,1)}, u32[]{:S(2)}, u32[]{:S(2)}) %all-to-all-start.1) | async-done | bytes 3145760 | tf_op jit(solution)/shard_map/all_to_all | solution.py:41
  265.6 2.5 reduce_sum.59
  268.1 1.2 fusion.35
  269.3 1.3 multiply_reduce_fusion.1
  270.7 2.0 add_convert_fusion.1
  272.6 0.0 all-gather.8.cloned.1.call-update
  272.7 0.0 reduce-scatter.2.cloned.1.call-start
  272.7 0.0 all-gather.12.cloned.1.call-done
  272.7 5.3 copy.22
  278.0 215.4 %all-gather.8.cloned.1.call-done = bf16[768,2048]{1,0:T(8,128)(2,1)} async-done(((bf16[96,2048]{1,0:T(8,128)(2,1)}), bf16[768,2048]{1,0:T(8,128)(2,1)}) %all-gather.8.cloned.1.call-update) | async-done | bytes 3145744 | tf_op jit(solution)/shard_map/all_gather | solution.py:153
  493.4 6.5 %fusion.29 = f32[768,704]{0,1:T(8,128)} fusion(bf16[768,2048]{1,0:T(8,128)(2,1)} %all-gather.8.cloned.1.call-done, bf16[2048,1408]{0,1:T(8,128)(2,1)} %all-gather.10.cloned.1.call-done), kind=kOutput, calls=%fused_computation.33 | convolution fusion | flops 2214592512 | bytes 8192000 | tf_op jit(solution)/shard_map/dot_general | solution.py:155
  499.9 12.5 %convolution_convert_fusion = bf16[768,2048]{1,0:T(8,128)(2,1)} fusion(bf16[88,8,16,128]{3,2,1,0:T(8,128)(2,1)} %bitcast.52, f32[768,704]{0,1:T(8,128)} %fusion.29, bf16[768,2048]{1,0:T(8,128)(2,1)} %all-gather.8.cloned.1.call-done, bf16[2048,1408]{0,1:T(8,128)(2,1)} %all-gather.10.cloned.1.call-done), kind=kOutput, calls=%fused_computation.27 | convolution fusion | flops 4434001920 | bytes 14221312 | tf_op jit(solution)/shard_map/dot_general | solution.py:158
  512.5 0.0 reduce-scatter.2.cloned.1.call-update
  512.5 36.1 %reduce-scatter.2.cloned.1.call-done = bf16[96,2048]{1,0:T(8,128)(2,1)} async-done(((bf16[768,2048]{1,0:T(8,128)(2,1)}), bf16[96,2048]{1,0:T(8,128)(2,1)}) %reduce-scatter.2.cloned.1.call-update) | async-done | bytes 393232 | tf_op jit(solution)/shard_map/reduce_scatter | solution.py:163
  548.6 1.2 fusion.36
  549.8 1.3 multiply_reduce_fusion
  551.1 2.0 add_convert_fusion
  (56 shorter events, 0.3 us)
Async XLA Ops:
  6.5 213.3 %copy-start = (bf16[256,2048]{1,0:T(8,128)(2,1)S(1)}, bf16[256,2048]{1,0:T(8,128)(2,1)}, u32[]{:S(2)}) copy-start(bf16[256,2048]{1,0:T(8,128)(2,1)} %param.22) | copy-start | bytes 3145732
  6.5 95.8 %all-gather.6.cloned.1.call-start = ((), (), s32[]{:S(2)}) async-start(), calls=%async_computation.3 | async-start | bytes 13369344 | tf_op jit(solution)/shard_map/all_gather | solution.py:31
  8.8 264.0 %all-gather.12.cloned.1.call-start = ((), (), s32[]{:S(2)}) async-start(), calls=%async_computation.7 | async-start | bytes 3063808 | tf_op jit(solution)/shard_map/all_gather | solution.py:160
  9.5 268.5 %all-gather.10.cloned.1.call-start = ((), (), s32[]{:S(2)}) async-start(), calls=%async_computation.5 | async-start | bytes 6127616 | tf_op jit(solution)/shard_map/all_gather | solution.py:31
  12.8 173.4 %all-to-all-start = ((f32[16,768,4]{1,2,0:T(4,128)}), f32[16,768,4]{1,2,0:T(4,128)S(1)}, u32[]{:S(2)}, u32[]{:S(2)}) async-start(f32[16,768,4]{1,2,0:T(4,128)} %broadcast_in_dim.56), calls=%async_computation | async-start | bytes 393216 | tf_op jit(solution)/shard_map/all_to_all | solution.py:18
  168.0 18.2 %copy-start.2 = (f32[768,4]{0,1:T(4,128)S(1)}, f32[768,4]{0,1:T(4,128)}, u32[]{:S(2)}) copy-start(f32[768,4]{0,1:T(4,128)} %param.20) | copy-start | bytes 36868
  222.6 48.0 %copy-start.3 = (f32[2048]{0:T(1024)S(1)}, f32[2048]{0:T(1024)}, u32[]{:S(2)}) copy-start(f32[2048]{0:T(1024)} %param.24) | copy-start | bytes 24580
  222.6 48.0 %copy-start.4 = (f32[2048]{0:T(1024)S(1)}, f32[2048]{0:T(1024)}, u32[]{:S(2)}) copy-start(f32[2048]{0:T(1024)} %param.23) | copy-start | bytes 24580
  222.6 43.0 %all-to-all-start.1 = ((bf16[8,96,2048]{2,1,0:T(8,128)(2,1)}), bf16[8,96,2048]{2,1,0:T(8,128)(2,1)}, u32[]{:S(2)}, u32[]{:S(2)}) async-start(bf16[8,96,2048]{2,1,0:T(8,128)(2,1)} %bitcast.50), calls=%async_computation.1 | async-start | bytes 6291456 | tf_op jit(solution)/shard_map/all_to_all | solution.py:41
  227.2 266.2 %all-gather.8.cloned.1.call-start = ((), (), s32[]{:S(2)}) async-start(), calls=%async_computation.4 | async-start | bytes 3538944 | tf_op jit(solution)/shard_map/all_gather | solution.py:153
  272.7 275.9 %reduce-scatter.2.cloned.1.call-start = ((), (), s32[]{:S(2)}) async-start(), calls=%async_computation.6 | async-start | bytes 3538944 | tf_op jit(solution)/shard_map/reduce_scatter | solution.py:163
  499.9 48.6 %copy-start.1 = (bf16[96,2048]{1,0:T(8,128)(2,1)S(1)}, bf16[96,2048]{1,0:T(8,128)(2,1)}, u32[]{:S(2)}) copy-start(bf16[96,2048]{1,0:T(8,128)(2,1)} %add_convert_fusion.1) | copy-start | bytes 1179652
  499.9 51.2 %copy-start.5 = (f32[2048]{0:T(1024)S(1)}, f32[2048]{0:T(1024)}, u32[]{:S(2)}) copy-start(f32[2048]{0:T(1024)} %param.29) | copy-start | bytes 24580
  499.9 51.2 %copy-start.6 = (f32[2048]{0:T(1024)S(1)}, f32[2048]{0:T(1024)}, u32[]{:S(2)}) copy-start(f32[2048]{0:T(1024)} %param.28) | copy-start | bytes 24580
Sparse Core Ops, SparseCore 0:
  9.5 92.8 all-gather.5
  104.5 46.6 all-gather.11
  153.3 63.4 all-gather.9
  272.8 220.5 all-gather.7
  512.6 35.9 reduce-scatter.1
